TPU v7x, 32 devices: a whole 2x2x4 slice. The times are simulated.
32 devices in a mesh: sp: 4 (over z), fs: 4 (over y, x), tp: 2 (over core).
Axes of the slice: x: 2, y: 2, z: 4, core: 2. Of those that a mesh axis runs over, the one named last changes fastest.
Arguments:
- hidden_in: bfloat16 [4, 1024, 2048], P('fs', 'sp', 'tp'), may hold values from -6 to 6
- sb_query_w: bfloat16 [2048, 1024], P('fs', 'tp'), may hold values from -0.21875 to 0.21875
- sb_key_w: bfloat16 [2048, 1024], P('fs', 'tp'), may hold values from -0.21875 to 0.21875
- sb_value_w: bfloat16 [2048, 1024], P('fs', 'tp'), may hold values from -0.125 to 0.125
- sb_offset: float32 [16], P('tp'), may hold values from -16 to -6
- delta_query_w: bfloat16 [2048, 1024], P('fs', 'tp'), may hold values from -0.125 to 0.125
- delta_key_w: bfloat16 [2048, 1024], P('fs', 'tp'), may hold values from -0.125 to 0.125
- delta_value_w: bfloat16 [2048, 1024], P('fs', 'tp'), may hold values from -0.125 to 0.125
- decay_w: bfloat16 [2048, 8], P(None, 'tp'), may hold values from -0.125 to 0.125
- write_w: bfloat16 [2048, 8], P(None, 'tp'), may hold values from -0.125 to 0.125
- write_bias: float32 [8], P('tp'), may hold values from -7 to 1.5
- decay_log_scale: float32 [8], P('tp'), may hold values from -14 to -3
- decay_shift: float32 [4, 8, 1024], P('fs', 'tp', 'sp'), may hold values from -3 to 0
- head_gain: float32 [128], replicated, may hold values from 0.1 to 1.9
- sb_out_w: bfloat16 [1024, 2048], P('tp'), may hold values from -0.125 to 0.125
- delta_out_w: bfloat16 [1024, 2048], P('tp'), may hold values from -0.125 to 0.125
Outputs:
- mixed_out: bfloat16 [4, 1024, 2048], P('fs', ('sp', 'tp'))
All inputs are finite; a program needn't handle non-finite values.
Results may differ from a plain program's by a relative error of at most 0.015.
Values may be sent and summed in bfloat16 or wider, within the bound.
A program may use at most 128 MiB of HBM per device.

v0:
```python
import jax
import jax.numpy as jnp
from jax import lax
from jax.sharding import PartitionSpec as P

SB_DIM = 64
GDN_DIM = 128
BLOCK = 64
EXACT_MATMUL = lax.Precision.HIGHEST
NORM_EPS = 1e-06


def carried_in(value, axis, combine, identity):
    devices, index = (lax.axis_size(axis), lax.axis_index(axis))
    everything = jax.tree.map(
        lambda part, kind: lax.all_gather(part.astype(kind), axis),
        value,
        (jnp.bfloat16, jnp.bfloat16),
    )
    start = jax.tree.map(
        lambda part, zero: jnp.broadcast_to(jnp.asarray(zero, part.dtype), part.shape),
        value,
        identity,
    )

    def lap(k, before):
        reached = k < index
        new = combine(
            before, jax.tree.map(lambda part, own: part[k].astype(own.dtype), everything, value)
        )
        return jax.tree.map(lambda a, b: jnp.where(reached, a, b), new, before)

    return lax.fori_loop(0, devices, lap, start)


def unit_lower_inverse(strict_part):
    order_size = strict_part.shape[-1]
    powered = strict_part
    inverse = jnp.eye(order_size, dtype=strict_part.dtype) - strict_part
    for repeat_number in range(max(1, (order_size - 1).bit_length()) - 1):
        powered = jnp.einsum("...ij,...jk->...ik", powered, powered, precision=EXACT_MATMUL)
        inverse = inverse + jnp.einsum(
            "...ij,...jk->...ik", inverse, powered, precision=EXACT_MATMUL
        )
    return inverse


def to_blocks(row_data, block_span):
    blocks_count = row_data.shape[0] // block_span
    shaped = row_data.reshape((blocks_count, block_span) + row_data.shape[1:])
    return jnp.swapaxes(shaped, 1, 2)


def from_blocks(blocked):
    swapped = jnp.swapaxes(blocked, 1, 2)
    return swapped.reshape((-1,) + swapped.shape[2:])


def unit_rows(vectors):
    return vectors * lax.rsqrt(jnp.sum(vectors * vectors, axis=-1, keepdims=True) + NORM_EPS)


def delta_inputs(
    query_proj,
    key_proj,
    value_proj,
    decay_pre,
    write_pre,
    write_bias,
    decay_log_scale,
    shift_rows,
    head_count,
    head_size,
):
    query_act = jax.nn.silu(query_proj.astype(jnp.float32)).reshape(-1, head_count, head_size)
    key_act = jax.nn.silu(key_proj.astype(jnp.float32)).reshape(-1, head_count, head_size)
    value_rows = jax.nn.silu(value_proj.astype(jnp.float32)).reshape(-1, head_count, head_size)
    queries = unit_rows(query_act) * head_size ** (-0.5)
    key_rows = unit_rows(key_act)
    log_decay = -jnp.exp(decay_log_scale) * jax.nn.softplus(decay_pre) + shift_rows
    strength = jax.nn.sigmoid(write_pre + write_bias)
    return (queries, key_rows, value_rows, log_decay, strength)


def delta_prepare(queries, key_rows, value_rows, log_decay, strength):
    block_span = queries.shape[2]
    cumulative = jnp.cumsum(log_decay, axis=-1)
    row_place = lax.broadcasted_iota(jnp.int32, (block_span, block_span), 0)
    col_place = lax.broadcasted_iota(jnp.int32, (block_span, block_span), 1)
    inclusive = col_place <= row_place
    strictly = col_place < row_place
    spread = cumulative[..., :, None] - cumulative[..., None, :]
    decay_table = jnp.where(inclusive, jnp.exp(jnp.where(inclusive, spread, 0.0)), 0.0)
    keys_beta = key_rows * strength[..., None]
    lower_part = jnp.where(
        strictly,
        jnp.einsum("nhik,nhjk->nhij", keys_beta, key_rows, precision=EXACT_MATMUL) * decay_table,
        0.0,
    )
    inverse = unit_lower_inverse(lower_part)
    growth = jnp.exp(cumulative)
    state_updates = jnp.einsum(
        "nhij,nhjv->nhiv", inverse, value_rows * strength[..., None], precision=EXACT_MATMUL
    )
    erase_term = jnp.einsum(
        "nhij,nhjk->nhik", inverse, keys_beta * growth[..., None], precision=EXACT_MATMUL
    )
    inside_block = (
        jnp.einsum("nhik,nhjk->nhij", queries, key_rows, precision=EXACT_MATMUL) * decay_table
    )
    boosted_query = queries * growth[..., None]
    damped_keys = key_rows * jnp.exp(cumulative[..., -1:] - cumulative)[..., None]
    decay_per_block = jnp.exp(cumulative[..., -1])
    return (state_updates, erase_term, inside_block, boosted_query, damped_keys, decay_per_block)


def delta_step(memory_state, inputs):
    state_updates, erase_term, inside_block, boosted_query, damped_keys, decay_per_block = inputs
    fixed_values = state_updates - jnp.einsum(
        "mzq,mqc->mzc", erase_term, memory_state, precision=EXACT_MATMUL
    )
    produced_rows = jnp.einsum(
        "mzq,mqc->mzc", boosted_query, memory_state, precision=EXACT_MATMUL
    ) + jnp.einsum("efq,eqn->efn", inside_block, fixed_values, precision=EXACT_MATMUL)
    memory_state = memory_state * decay_per_block[:, None, None] + jnp.einsum(
        "wam,waz->wmz", damped_keys, fixed_values, precision=EXACT_MATMUL
    )
    return (memory_state, produced_rows)


def transition_step(carried, inputs):
    memory_state, transfer = carried
    state_updates, erase_term, inside_block, boosted_query, damped_keys, decay_per_block = inputs
    fixed_values = state_updates - jnp.einsum(
        "mzq,mqc->mzc", erase_term, memory_state, precision=EXACT_MATMUL
    )
    coupling = jnp.einsum("hik,hil->hkl", damped_keys, erase_term, precision=EXACT_MATMUL)
    memory_state = memory_state * decay_per_block[:, None, None] + jnp.einsum(
        "wam,waz->wmz", damped_keys, fixed_values, precision=EXACT_MATMUL
    )
    transfer = transfer * decay_per_block[:, None, None] - jnp.einsum(
        "hkl,hlm->hkm", coupling, transfer, precision=EXACT_MATMUL
    )
    return ((memory_state, transfer), None)


def compose(prior_blocks, following_blocks):
    joined_map = jnp.einsum(
        "hkl,hlm->hkm", following_blocks[0], prior_blocks[0], precision=EXACT_MATMUL
    )
    joined_state = (
        jnp.einsum("djo,dog->djg", following_blocks[0], prior_blocks[1], precision=EXACT_MATMUL)
        + following_blocks[1]
    )
    return (joined_map, joined_state)


def stick_block(queries, key_rows, value_rows, query_place, key_place, offsets):
    scale_factor = queries.shape[-1] ** (-0.5)
    scores = (
        jnp.einsum("qhd,khd->hqk", queries, key_rows, preferred_element_type=jnp.float32)
        * scale_factor
        + offsets[:, None, None]
    )
    visible = key_place[None, :] < query_place[:, None]
    skipped = jnp.where(visible, jax.nn.log_sigmoid(-scores), 0.0)
    beyond = lax.cumsum(skipped, axis=2, reverse=True) - skipped
    weights = jnp.where(visible, jnp.exp(jax.nn.log_sigmoid(scores) + beyond), 0.0).astype(
        jnp.bfloat16
    )
    partial_value = jnp.einsum(
        "hqk,khd->qhd", weights, value_rows, preferred_element_type=jnp.float32
    )
    return (partial_value, jnp.sum(skipped, axis=2).T)


def stick_combine(partials, totals):
    beyond = jnp.cumsum(totals[::-1], axis=0)[::-1] - totals
    return jnp.sum(partials * jnp.exp(beyond)[..., None], axis=0)


def on_device(
    hidden_in,
    sb_query_w,
    sb_key_w,
    sb_value_w,
    sb_offset,
    delta_query_w,
    delta_key_w,
    delta_value_w,
    decay_w,
    write_w,
    write_bias,
    decay_log_scale,
    decay_shift,
    head_gain,
    sb_out_w,
    delta_out_w,
):
    token_rows = hidden_in.shape[1]
    local_in = hidden_in.reshape(token_rows, hidden_in.shape[2])
    gathered = (
        lax.all_gather(sb_query_w, "fs", axis=0, tiled=True),
        lax.all_gather(sb_key_w, "fs", axis=0, tiled=True),
        lax.all_gather(sb_value_w, "fs", axis=0, tiled=True),
        lax.all_gather(delta_query_w, "fs", axis=0, tiled=True),
        lax.all_gather(delta_key_w, "fs", axis=0, tiled=True),
        lax.all_gather(delta_value_w, "fs", axis=0, tiled=True),
    )
    in_weights = tuple(gathered) + (decay_w, write_w)
    portion = lax.all_gather(local_in, "tp", axis=1, tiled=True)
    projected = tuple(
        (jnp.dot(portion, weight, preferred_element_type=jnp.float32) for weight in in_weights)
    )
    sb_heads = sb_offset.shape[0]
    delta_heads = decay_log_scale.shape[0]
    sb_query = projected[0].astype(jnp.bfloat16).reshape(token_rows, sb_heads, SB_DIM)
    sb_keys = projected[1].astype(jnp.bfloat16)
    sb_values = projected[2].astype(jnp.bfloat16)
    shift_rows = decay_shift.reshape(delta_heads, token_rows).T
    queries, key_rows, value_rows, log_decay, strength = delta_inputs(
        projected[3].astype(jnp.bfloat16),
        projected[4].astype(jnp.bfloat16),
        projected[5].astype(jnp.bfloat16),
        projected[6],
        projected[7],
        write_bias,
        decay_log_scale,
        shift_rows,
        delta_heads,
        GDN_DIM,
    )
    prepared = delta_prepare(
        to_blocks(queries, BLOCK),
        to_blocks(key_rows, BLOCK),
        to_blocks(value_rows, BLOCK),
        to_blocks(log_decay, BLOCK),
        to_blocks(strength, BLOCK),
    )
    identity_map = jnp.broadcast_to(
        jnp.eye(GDN_DIM, dtype=jnp.float32), (delta_heads, GDN_DIM, GDN_DIM)
    )
    empty_state = jnp.zeros((delta_heads, GDN_DIM, GDN_DIM), jnp.float32)
    (local_end, local_map), unused_out = lax.scan(
        transition_step, (empty_state, identity_map), prepared
    )
    own_first = lax.axis_index("sp") * token_rows
    query_place = own_first + lax.iota(jnp.int32, token_rows)
    sp_count = lax.axis_size("sp")
    slot_out = jnp.zeros((sp_count, token_rows, sb_heads, SB_DIM), jnp.float32)
    slot_total = jnp.zeros((sp_count, token_rows, sb_heads), jnp.float32)

    def absorb(slot_arrays, address_portion, value_part, shard_first):

        def active(current):
            partial_value, totals = stick_block(
                sb_query,
                address_portion.reshape(token_rows, sb_heads, SB_DIM),
                value_part.reshape(token_rows, sb_heads, SB_DIM),
                query_place,
                shard_first + lax.iota(jnp.int32, token_rows),
                sb_offset,
            )
            slot_index = shard_first // token_rows
            return (
                lax.dynamic_update_index_in_dim(current[0], partial_value, slot_index, 0),
                lax.dynamic_update_index_in_dim(current[1], totals, slot_index, 0),
            )

        def inactive(current):
            return current

        usable = jnp.logical_and(shard_first >= 0, shard_first <= own_first)
        return lax.cond(usable, active, inactive, slot_arrays)

    key_block = lax.all_gather(sb_keys, "sp", axis=0, tiled=True)
    value_block = lax.all_gather(sb_values, "sp", axis=0, tiled=True)

    def per_shard(shard_number, current):
        row_begin = shard_number * token_rows
        return absorb(
            current,
            lax.dynamic_slice_in_dim(key_block, row_begin, token_rows, 0),
            lax.dynamic_slice_in_dim(value_block, row_begin, token_rows, 0),
            row_begin,
        )

    slot_arrays = lax.fori_loop(
        0, key_block.shape[0] // token_rows, per_shard, (slot_out, slot_total)
    )
    unused_map, incoming = carried_in(
        (local_map, local_end), "sp", compose, (identity_map, empty_state)
    )
    sb_mixed = (
        stick_combine(slot_arrays[0], slot_arrays[1])
        .astype(jnp.bfloat16)
        .reshape(token_rows, sb_heads * SB_DIM)
    )
    unused_end, produced_rows = lax.scan(delta_step, incoming, prepared)
    produced_rows = from_blocks(produced_rows)
    normed = (
        produced_rows
        * lax.rsqrt(jnp.mean(produced_rows * produced_rows, axis=-1, keepdims=True) + NORM_EPS)
        * head_gain
    )
    delta_mixed = normed.astype(jnp.bfloat16).reshape(token_rows, delta_heads * GDN_DIM)
    result = lax.psum_scatter(
        (
            jnp.dot(sb_mixed, sb_out_w, preferred_element_type=jnp.float32)
            + jnp.dot(delta_mixed, delta_out_w, preferred_element_type=jnp.float32)
        ).astype(jnp.bfloat16),
        "tp",
        scatter_dimension=0,
        tiled=True,
    ).astype(jnp.float32)
    return result.astype(jnp.bfloat16).reshape(1, result.shape[0], result.shape[1])


def solution(mesh):
    return jax.shard_map(
        on_device,
        mesh=mesh,
        in_specs=(
            P("fs", "sp", "tp"),
            P("fs", "tp"),
            P("fs", "tp"),
            P("fs", "tp"),
            P("tp"),
            P("fs", "tp"),
            P("fs", "tp"),
            P("fs", "tp"),
            P(None, "tp"),
            P(None, "tp"),
            P("tp"),
            P("tp"),
            P("fs", "tp", "sp"),
            P(),
            P("tp", None),
            P("tp", None),
        ),
        out_specs=P("fs", ("sp", "tp"), None),
        check_vma=False,
    )
```

profile of v0, /device:TPU:0, one launch (start us, length us, event | category | flops | bytes accessed | tf_op | source)
XLA Modules:
  0.0 387.4 jit_solution(17021583337816945138)
XLA Ops:
  12.1 8.6 %all-gather.29.cloned.1.call-done = bf16[1,256,2048]{2,1,0:T(8,128)(2,1)} async-done(((bf16[1,256,1024]{2,1,0:T(8,128)(2,1)}), bf16[1,256,2048]{2,1,0:T(8,128)(2,1)}) %all-gather.29.cloned.1.call-update) | async-done | bytes 1048592 | tf_op jit(solution)/shard_map/all_gather | solution.py:211
  25.4 33.6 %all-gather.23.cloned.1.call-done = bf16[2048,512]{1,0:T(8,128)(2,1)} async-done(((bf16[512,512]{1,0:T(8,128)(2,1)}), bf16[2048,512]{1,0:T(8,128)(2,1)}) %all-gather.23.cloned.1.call-update) | async-done | bytes 2097168 | tf_op jit(solution)/shard_map/all_gather | solution.py:207
  58.9 3.7 fusion.116
  74.3 21.7 %all-gather.25.cloned.1.call-done = bf16[2048,512]{1,0:T(8,128)(2,1)} async-done(((bf16[512,512]{1,0:T(8,128)(2,1)}), bf16[2048,512]{1,0:T(8,128)(2,1)}) %all-gather.25.cloned.1.call-update) | async-done | bytes 2097168 | tf_op jit(solution)/shard_map/all_gather | solution.py:208
  96.0 3.5 divide_multiply_fusion.1
  99.5 2.0 reshape_reshape.3
  103.5 2.1 fusion.78
  107.1 25.7 %all-gather.27.cloned.1.call-done = bf16[2048,512]{1,0:T(8,128)(2,1)} async-done(((bf16[512,512]{1,0:T(8,128)(2,1)}), bf16[2048,512]{1,0:T(8,128)(2,1)}) %all-gather.27.cloned.1.call-update) | async-done | bytes 2097168 | tf_op jit(solution)/shard_map/all_gather | solution.py:206
  132.9 3.8 fusion.117
  140.3 2.1 reshape.155
  142.3 2.9 bitcast_multiply_fusion.1
  145.3 19.1 %while.57 = (s32[]{:T(128)}, f32[4,128,128]{2,1,0:T(8,128)S(1)}, f32[4,128,128]{2,1,0:T(8,128)S(1)}, f32[4,4]{1,0:T(4,128)S(1)}, f32[4,4,64,128]{3,2,1,0:T(8,128...) while((s32[]{:T(128)}, f32[4,128,128]{2,1,0:T(8,128)S(1)}, ...), condition=%wide.region_12.13_spmd.clone, body=%wide.region_11.12_spmd.clone.sunk | while | flops 252084224 | bytes 3279532 | solution.py:244
  165.0 16.0 %all-gather.1 = bf16[16,128,128]{2,1,0:T(8,128)(2,1)} all-gather(bf16[4,128,128]{2,1,0:T(8,128)(2,1)S(1)} %convert_element_type.96), channel_id=3, replica_groups=mesh['sp'=4,'fs'=4,'tp'=2] {'sp'}, dimensions={0}, use_global_device_ids=true | all-gather | bytes 655360 | tf_op jit(solution)/shard_map/all_gather | solution.py:16
  180.9 3.4 convolution_convert_fusion.5
  184.4 17.0 %all-gather.2 = bf16[16,128,128]{2,1,0:T(8,128)(2,1)} all-gather(bf16[4,128,128]{2,1,0:T(8,128)(2,1)S(1)} %convert_element_type.97), channel_id=4, replica_groups=mesh['sp'=4,'fs'=4,'tp'=2] {'sp'}, dimensions={0}, use_global_device_ids=true | all-gather | bytes 655360 | tf_op jit(solution)/shard_map/all_gather | solution.py:16
  201.4 3.0 convolution_multiply_fusion
  204.5 2.2 all-gather.19.cloned.1.call-done
  206.7 3.3 convolution_convert_fusion.3
  210.0 5.3 %while.58 = (s32[]{:T(128)}, f32[4,128,128]{2,1,0:T(8,128)S(1)}, s32[]{:T(128)}, bf16[4,4,128,128]{3,2,1,0:T(8,128)(2,1)}, bf16[4,4,128,128]{3,2,1,0:T(8,128)(2,1)}, /*index=5*/s32[]{:T(128)}, s32[]{:T(128)}) while((s32[]{:T(128)}, f32[4,128,128]{2,1,0:T(8,128)S(1)}, s32[]{:T(128)}, bf16[4,4,128,128]{3,2,1,0:T(8,128)(2,1)}, ...), condition=%wide.region_14.15_spmd.clone, body=%wide.region_13.14_spmd.clone.sunk | while | flops 100990976 | bytes 1575519 | solution.py:33
  215.4 23.9 %while.56 = (s32[]{:T(128)}, f32[4,128,128]{2,1,0:T(8,128)S(1)}, f32[4,4,64,128]{3,2,1,0:T(8,128)S(1)}, f32[4,4]{1,0:T(4,128)}, f32[4,4,64,128]{3,2,1,0:T(8,128)...) while((s32[]{:T(128)}, f32[4,128,128]{2,1,0:T(8,128)S(1)}, ...), condition=%wide.region_17.18_spmd, body=%wide.region_16.17_spmd.sunk | while | flops 176357376 | bytes 2493593 | solution.py:299
  240.8 2.9 all-gather.17.cloned.1.call-done
  243.7 2.6 convolution_convert_fusion.4
  247.2 26.1 %all-gather.15.cloned.1.call-done = bf16[1024,512]{1,0:T(8,128)(2,1)} async-done(((bf16[256,512]{1,0:T(8,128)(2,1)}), bf16[1024,512]{1,0:T(8,128)(2,1)}) %all-gather.15.cloned.1.call-update) | async-done | bytes 1048592 | tf_op jit(solution)/shard_map/all_gather | solution.py:276
  273.3 2.3 copy.80
  275.6 26.7 %all-gather.21.cloned.1.call-done = bf16[1024,512]{1,0:T(8,128)(2,1)} async-done(((bf16[256,512]{1,0:T(8,128)(2,1)}), bf16[1024,512]{1,0:T(8,128)(2,1)}) %all-gather.21.cloned.1.call-update) | async-done | bytes 1048592 | tf_op jit(solution)/shard_map/all_gather | solution.py:277
  302.3 2.3 copy.81
  306.8 14.7 %while.59 = (s32[]{:T(128)}, f32[4,256,8,64]{1,3,2,0:T(8,128)}, f32[4,256,8]{1,2,0:T(8,128)}, s32[]{:T(128)}, bf16[1024,512]{0,1:T(8,128)(2,1)}, /*index=5*/bf16...) while((s32[]{:T(128)}, f32[4,256,8,64]{1,3,2,0:T(8,128)}, ...), condition=%wide.region_6.7_spmd.clone.clone, body=%wide.region_0.6_spmd.clone.clone.sunk | while | flops 218698256 | bytes 25745960 | solution.py:288
  306.8 14.7 %conditional.4 = ((f32[4,256,8,64]{1,3,2,0:T(8,128)}, f32[4,256,8]{1,2,0:T(8,128)})) conditional(s32[]{:T(128)} %convert_element_type.140, (f32[4,256,8,64]{1,3,2,0:T(8,128)}, f32[4,256,8]{1,2,0:T(8,128)}) %tuple.124, (s32[]{:T(128)}, s32[]{:T(128)}, bf16[1024,512]{0,1:T(8,128)(2,1)}, bf16[256,8,64]{0,2,1:T(8,128)(2,1)}, f32[8]{0:T(128)S(1)}, ...), branch_computations={%region_1.1_spmd, %region_2.0_spmd} | conditional | flops 218698256 | bytes 25744700 | solution.py:274
  308.0 2.7 fusion.17
  310.7 5.1 %fusion.13 = f32[8,256,2,128]{1,0,3,2:T(8,128)S(1)} fusion(f32[8,256,2,128]{1,3,2,0:T(8,128)S(1)} %bitcast.258), kind=kOutput, calls=%fused_computation.18 | output fusion | flops 66584576 | bytes 4194304 | tf_op jit(solution)/shard_map/reduce-window.6
  316.7 3.0 fusion.6
  328.6 51.9 %reduce-scatter.2.cloned.1.call-done = bf16[128,2048]{1,0:T(8,128)(2,1)} async-done(((bf16[256,2048]{1,0:T(8,128)(2,1)}), bf16[128,2048]{1,0:T(8,128)(2,1)}) %reduce-scatter.2.cloned.1.call-update) | async-done | bytes 524304 | tf_op jit(solution)/shard_map/reduce_scatter | solution.py:307
  (184 shorter events, 92.5 us)
Async XLA Ops:
  6.5 318.5 %copy-start = (bf16[512,2048]{1,0:T(8,128)(2,1)S(1)}, bf16[512,2048]{1,0:T(8,128)(2,1)}, u32[]{:S(2)}) copy-start(bf16[512,2048]{1,0:T(8,128)(2,1)} %param.40) | copy-start | bytes 6291460
  6.5 4.9 %copy-start.18 = (f32[4]{0:T(128)S(1)}, f32[4]{0:T(128)}, u32[]{:S(2)}) copy-start(f32[4]{0:T(128)} %param.37) | copy-start | bytes 52
  6.5 4.9 %copy-start.17 = (f32[128]{0:T(128)S(1)}, f32[128]{0:T(128)}, u32[]{:S(2)}) copy-start(f32[128]{0:T(128)} %param.39) | copy-start | bytes 1540
  6.5 14.1 %copy-start.9 = (bf16[2048,4]{0,1:T(4,128)(2,1)S(1)}, bf16[2048,4]{0,1:T(4,128)(2,1)}, u32[]{:S(2)}) copy-start(bf16[2048,4]{0,1:T(4,128)(2,1)} %param.34) | copy-start | bytes 49156
  6.5 14.1 %copy-start.14 = (f32[1,4,256]{2,1,0:T(4,128)S(1)}, f32[1,4,256]{2,1,0:T(4,128)}, u32[]{:S(2)}) copy-start(f32[1,4,256]{2,1,0:T(4,128)} %param.38) | copy-start | bytes 12292
  6.5 14.1 %all-gather.29.cloned.1.call-start = ((), (), s32[]{:S(2)}) async-start(), calls=%async_computation.10 | async-start | bytes 1572864 | tf_op jit(solution)/shard_map/all_gather | solution.py:211
  7.3 16.3 %copy-start.10 = (bf16[2048,4]{0,1:T(4,128)(2,1)S(1)}, bf16[2048,4]{0,1:T(4,128)(2,1)}, u32[]{:S(2)}) copy-start(bf16[2048,4]{0,1:T(4,128)(2,1)} %param.35) | copy-start | bytes 49156
  7.3 16.3 %copy-start.16 = (f32[4]{0:T(128)S(1)}, f32[4]{0:T(128)}, u32[]{:S(2)}) copy-start(f32[4]{0:T(128)} %param.36) | copy-start | bytes 52
  7.3 51.6 %all-gather.23.cloned.1.call-start = ((), (), s32[]{:S(2)}) async-start(), calls=%async_computation.6 | async-start | bytes 2621440 | tf_op jit(solution)/shard_map/all_gather | solution.py:207
  8.1 87.9 %all-gather.25.cloned.1.call-start = ((), (), s32[]{:S(2)}) async-start(), calls=%async_computation.7 | async-start | bytes 2621440 | tf_op jit(solution)/shard_map/all_gather | solution.py:208
  8.8 124.1 %all-gather.27.cloned.1.call-start = ((), (), s32[]{:S(2)}) async-start(), calls=%async_computation.8 | async-start | bytes 2621440 | tf_op jit(solution)/shard_map/all_gather | solution.py:206
  9.4 171.6 %all-gather.13.cloned.1.call-start = ((), (), s32[]{:S(2)}) async-start(), calls=%async_computation.1 | async-start | bytes 2621440 | tf_op jit(solution)/shard_map/all_gather | solution.py:204
  10.0 196.7 %all-gather.19.cloned.1.call-start = ((), (), s32[]{:S(2)}) async-start(), calls=%async_computation.4 | async-start | bytes 2621440 | tf_op jit(solution)/shard_map/all_gather | solution.py:205
  10.5 233.2 %all-gather.17.cloned.1.call-start = ((), (), s32[]{:S(2)}) async-start(), calls=%async_computation.3 | async-start | bytes 2621440 | tf_op jit(solution)/shard_map/all_gather | solution.py:203
  11.3 262.0 %all-gather.15.cloned.1.call-start = ((), (), s32[]{:S(2)}) async-start(), calls=%async_computation.2 | async-start | bytes 1310720 | tf_op jit(solution)/shard_map/all_gather | solution.py:276
  11.3 54.2 %copy-start.13 = (pred[64,64]{1,0:T(8,128)(4,1)}, pred[64,64]{1,0:T(8,128)(4,1)S(1)}, u32[]{:S(2)}) copy-start(pred[64,64]{1,0:T(8,128)(4,1)S(1)} %iota_compare_fusion.1) | copy-start | bytes 12292
  65.5 1.3 copy-start.1
  74.3 27.2 %copy-start.3 = (f32[4,4,64,64]{3,2,1,0:T(8,128)S(1)}, f32[4,4,64,64]{3,2,1,0:T(8,128)}, u32[]{:S(2)}) copy-start(f32[4,4,64,64]{3,2,1,0:T(8,128)} %fusion.124) | copy-start | bytes 786436
  101.5 4.0 %copy-start.5 = (f32[4,64,4,128]{3,2,1,0:T(4,128)S(1)}, f32[4,64,4,128]{3,2,1,0:T(4,128)}, u32[]{:S(2)}) copy-start(f32[4,64,4,128]{3,2,1,0:T(4,128)} %reshape_reshape.3) | copy-start | bytes 1572868
  140.3 5.0 %copy-start.8 = (f32[4,64,4]{1,2,0:T(4,128)}, f32[4,64,4]{1,2,0:T(4,128)S(1)}, u32[]{:S(2)}) copy-start(f32[4,64,4]{1,2,0:T(4,128)S(1)} %copy.89) | copy-start | bytes 12292
  164.4 0.6 copy-start.15
  180.9 20.5 %copy-start.2 = (f32[4,64,4,128]{3,2,1,0:T(4,128)S(1)}, f32[4,64,4,128]{3,2,1,0:T(4,128)}, u32[]{:S(2)}) copy-start(f32[4,64,4,128]{3,2,1,0:T(4,128)} %copy-done.1) | copy-start | bytes 1572868
  184.3 118.0 %all-gather.21.cloned.1.call-start = ((), (), s32[]{:S(2)}) async-start(), calls=%async_computation.5 | async-start | bytes 1310720 | tf_op jit(solution)/shard_map/all_gather | solution.py:277
  210.0 5.4 %copy-start.7 = (f32[4,4,64,128]{3,2,1,0:T(8,128)S(1)}, f32[4,4,64,128]{3,2,1,0:T(8,128)}, u32[]{:S(2)}) copy-start(f32[4,4,64,128]{3,2,1,0:T(8,128)} %custom-call.2) | copy-start | bytes 1572868
  215.4 165.2 %reduce-scatter.2.cloned.1.call-start = ((), (), s32[]{:S(2)}) async-start(), calls=%async_computation.9 | async-start | bytes 1572864 | tf_op jit(solution)/shard_map/reduce_scatter | solution.py:307
  275.6 31.2 %copy-start.11 = (f32[8]{0:T(128)S(1)}, f32[8]{0:T(128)}, u32[]{:S(2)}) copy-start(f32[8]{0:T(128)} %param.30) | copy-start | bytes 100
  325.1 1.1 copy-start.4
  325.1 1.8 copy-start.6
  325.1 1.8 copy-start.12
Sparse Core Ops, SparseCore 0:
  8.9 11.7 all-gather.28
  22.5 36.3 all-gather.22
  60.8 35.1 all-gather.24
  97.7 35.1 all-gather.26
  134.6 35.1 all-gather.12
  171.5 35.1 all-gather.18
  208.5 35.1 all-gather.16
  245.3 27.9 all-gather.14
  274.9 27.3 all-gather.20
  328.7 51.7 reduce-scatter.1
where the time goes:
time: 389 us; the launch traced here: 387 us
  waiting for transfers between devices  204 us (52%)
  matrix products  92.1 us (24%)
  blocking collectives  33 us (8%)
  local copies, waits for them, and re-layouts  26.2 us (7%)
  other arithmetic  17.2 us (4%)
  between operations  14 us (4%)
    reduce_scatter x1, waiting for transfers between devices, on_device(): lax.psum_scatter((jnp.dot(sb_mixed, sb_out_w, preferred_element_type=jnp....  51.9 us
    all_gather x1, waiting for transfers between devices, on_device(): lax.all_gather(delta_key_w, 'fs', axis=0, tiled=True)  33.6 us
    all_gather x2, blocking collectives, carried_in(): lax.all_gather(part.astype(kind), axis)  33 us
    all_gather x1, waiting for transfers between devices, on_device(): value_block = lax.all_gather(sb_values, 'sp', axis=0, tiled=True)  26.7 us
    all_gather x1, waiting for transfers between devices, on_device(): key_block = lax.all_gather(sb_keys, 'sp', axis=0, tiled=True)  26.1 us
    all_gather x1, waiting for transfers between devices, on_device(): lax.all_gather(delta_query_w, 'fs', axis=0, tiled=True)  25.7 us
    dot_general x8, matrix products, on_device(): jnp.dot(portion, weight, preferred_element_type=jnp.float32)  23.6 us
    all_gather x1, waiting for transfers between devices, on_device(): lax.all_gather(delta_value_w, 'fs', axis=0, tiled=True)  21.7 us
  transfers between devices with their start and end apart: 10, of which 9 were waited for; matrix products, arithmetic and copies ran while one was open for 28% of the time, Pallas kernels for 0%

commit v1 on v0

--- a/solution.py
+++ b/solution.py
@@ -273,7 +273,13 @@
         usable = jnp.logical_and(shard_first >= 0, shard_first <= own_first)
         return lax.cond(usable, active, inactive, slot_arrays)
 
-    key_block = lax.all_gather(sb_keys, "sp", axis=0, tiled=True)
+    peers = lax.axis_size("sp")
+    block, blocks = (sb_keys, [sb_keys])
+    for _ in range(peers - 1):
+        block = lax.ppermute(block, "sp", [(i, (i + 1) % peers) for i in range(peers)])
+        blocks.insert(0, block)
+    merged = jnp.concatenate(blocks, axis=0)
+    key_block = jnp.roll(merged, (lax.axis_index("sp") + 1) * sb_keys.shape[0], axis=0)
     value_block = lax.all_gather(sb_values, "sp", axis=0, tiled=True)
 
     def per_shard(shard_number, current):

time: 389 us -> 360 us (0.925)
  waiting for transfers between devices: 204 us -> 168 us
    all_gather x1 -> x0, waiting for transfers between devices: 26.1 us -> none  [on_device(): key_block = lax.all_gather(sb_keys, 'sp', axis=0, tiled=True)]
    all_gather x1, waiting for transfers between devices: 26.7 us -> 11.1 us  [on_device(): value_block = lax.all_gather(sb_values, 'sp', axis=0, tiled=True)]
    ppermute x0 -> x3, waiting for transfers between devices: none -> 10.3 us  [on_device(): lax.ppermute(block, 'sp', [(i, (i + 1) % peers) for i in range(peers)])]
    unnamed x40 -> x41, local copies, waits for them, and re-layouts: 5.82 us -> 10.4 us
  transfers between devices with their start and end apart: 10 -> 12, of which waited for: 9 -> 8; matrix products, arithmetic and copies ran while one was open for 28% -> 32% of each run, Pallas kernels for 0% -> 0%
where the time goes in v1:
time: 360 us; the launch traced here: 358 us
  waiting for transfers between devices  168 us (47%)
  matrix products  93.8 us (26%)
  blocking collectives  33.2 us (9%)
  local copies, waits for them, and re-layouts  30 us (8%)
  other arithmetic  16.9 us (5%)
  between operations  13.7 us (4%)
    reduce_scatter x1, waiting for transfers between devices, on_device(): lax.psum_scatter((jnp.dot(sb_mixed, sb_out_w, preferred_element_type=jnp....  51.9 us
    all_gather x1, waiting for transfers between devices, on_device(): lax.all_gather(delta_key_w, 'fs', axis=0, tiled=True)  33.6 us
    all_gather x2, blocking collectives, carried_in(): lax.all_gather(part.astype(kind), axis)  33.2 us
    all_gather x1, waiting for transfers between devices, on_device(): lax.all_gather(delta_query_w, 'fs', axis=0, tiled=True)  25.8 us
    dot_general x8, matrix products, on_device(): jnp.dot(portion, weight, preferred_element_type=jnp.float32)  23.3 us
    all_gather x1, waiting for transfers between devices, on_device(): lax.all_gather(delta_value_w, 'fs', axis=0, tiled=True)  22.5 us
    all_gather x1, waiting for transfers between devices, on_device(): value_block = lax.all_gather(sb_values, 'sp', axis=0, tiled=True)  11.1 us
    unnamed x41, local copies, waits for them, and re-layouts  10.4 us
  transfers between devices with their start and end apart: 12, of which 8 were waited for; matrix products, arithmetic and copies ran while one was open for 32% of the time, Pallas kernels for 0%

profile of v1, /device:TPU:0, one launch (start us, length us, event | category | flops | bytes accessed | tf_op | source)
XLA Modules:
  0.0 358.1 jit_solution(10006473722620727908)
XLA Ops:
  12.1 8.6 %all-gather.26.cloned.1.call-done = bf16[1,256,2048]{2,1,0:T(8,128)(2,1)} async-done(((bf16[1,256,1024]{2,1,0:T(8,128)(2,1)}), bf16[1,256,2048]{2,1,0:T(8,128)(2,1)}) %all-gather.26.cloned.1.call-update) | async-done | bytes 1048592 | tf_op jit(solution)/shard_map/all_gather | solution.py:211
  25.4 33.6 %all-gather.20.cloned.1.call-done = bf16[2048,512]{1,0:T(8,128)(2,1)} async-done(((bf16[512,512]{1,0:T(8,128)(2,1)}), bf16[2048,512]{1,0:T(8,128)(2,1)}) %all-gather.20.cloned.1.call-update) | async-done | bytes 2097168 | tf_op jit(solution)/shard_map/all_gather | solution.py:207
  58.9 3.7 %fusion.116 = (f32[256,512]{1,0:T(8,128)}, f32[256,512]{1,0:T(8,128)}) fusion(bf16[2048,512]{1,0:T(8,128)(2,1)} %all-gather.20.cloned.1.call-done, bf16[1,256,2048]{2,1,0:T(8,128)(2,1)} %all-gather.26.cloned.1.call-done), kind=kOutput, calls=%fused_computation.181 | convolution fusion | flops 537788416 | bytes 4194304 | tf_op jit(solution)/shard_map/dot_general | solution.py:213
  73.5 22.5 %all-gather.22.cloned.1.call-done = bf16[2048,512]{1,0:T(8,128)(2,1)} async-done(((bf16[512,512]{1,0:T(8,128)(2,1)}), bf16[2048,512]{1,0:T(8,128)(2,1)}) %all-gather.22.cloned.1.call-update) | async-done | bytes 2097168 | tf_op jit(solution)/shard_map/all_gather | solution.py:208
  96.0 3.5 divide_multiply_fusion.1
  99.5 2.0 reshape_reshape.3
  103.4 2.1 fusion.78
  107.1 25.8 %all-gather.24.cloned.1.call-done = bf16[2048,512]{1,0:T(8,128)(2,1)} async-done(((bf16[512,512]{1,0:T(8,128)(2,1)}), bf16[2048,512]{1,0:T(8,128)(2,1)}) %all-gather.24.cloned.1.call-update) | async-done | bytes 2097168 | tf_op jit(solution)/shard_map/all_gather | solution.py:206
  132.9 3.9 %fusion.117 = (f32[256,512]{1,0:T(8,128)}, f32[256,512]{1,0:T(8,128)}) fusion(bf16[2048,512]{1,0:T(8,128)(2,1)} %all-gather.24.cloned.1.call-done, bf16[1,256,2048]{2,1,0:T(8,128)(2,1)} %all-gather.26.cloned.1.call-done), kind=kOutput, calls=%fused_computation.182 | convolution fusion | flops 537788416 | bytes 4194304 | tf_op jit(solution)/shard_map/dot_general | solution.py:213
  136.7 2.0 mul.201
  140.3 2.0 reshape.155
  142.3 3.4 convolution_multiply_fusion
  147.3 19.1 %while.57 = (s32[]{:T(128)}, f32[4,128,128]{2,1,0:T(8,128)S(1)}, f32[4,128,128]{2,1,0:T(8,128)S(1)}, f32[4,4]{1,0:T(4,128)S(1)}, f32[4,4,64,128]{3,2,1,0:T(8,128...) while((s32[]{:T(128)}, f32[4,128,128]{2,1,0:T(8,128)S(1)}, ...), condition=%wide.region_12.13_spmd.clone, body=%wide.region_11.12_spmd.clone.sunk | while | flops 252084224 | bytes 3279532 | solution.py:244
  166.4 16.0 %all-gather.1 = bf16[16,128,128]{2,1,0:T(8,128)(2,1)} all-gather(bf16[4,128,128]{2,1,0:T(8,128)(2,1)S(1)} %convert_element_type.96), channel_id=3, replica_groups=mesh['sp'=4,'fs'=4,'tp'=2] {'sp'}, dimensions={0}, use_global_device_ids=true | all-gather | bytes 655360 | tf_op jit(solution)/shard_map/all_gather | solution.py:16
  182.5 17.1 %all-gather.2 = bf16[16,128,128]{2,1,0:T(8,128)(2,1)} all-gather(bf16[4,128,128]{2,1,0:T(8,128)(2,1)S(1)} %convert_element_type.97), channel_id=4, replica_groups=mesh['sp'=4,'fs'=4,'tp'=2] {'sp'}, dimensions={0}, use_global_device_ids=true | all-gather | bytes 655360 | tf_op jit(solution)/shard_map/all_gather | solution.py:16
  199.6 5.2 %while.58 = (s32[]{:T(128)}, f32[4,128,128]{2,1,0:T(8,128)S(1)}, s32[]{:T(128)}, bf16[4,4,128,128]{3,2,1,0:T(8,128)(2,1)}, bf16[4,4,128,128]{3,2,1,0:T(8,128)(2,1)}, /*index=5*/s32[]{:T(128)}, s32[]{:T(128)}) while((s32[]{:T(128)}, f32[4,128,128]{2,1,0:T(8,128)S(1)}, s32[]{:T(128)}, bf16[4,4,128,128]{3,2,1,0:T(8,128)(2,1)}, ...), condition=%wide.region_14.15_spmd.clone, body=%wide.region_13.14_spmd.clone.sunk | while | flops 100990976 | bytes 1575519 | solution.py:33
  204.9 2.6 convolution_convert_fusion.5
  208.5 23.7 %while.56 = (s32[]{:T(128)}, f32[4,128,128]{2,1,0:T(8,128)S(1)}, f32[4,4,64,128]{3,2,1,0:T(8,128)}, f32[4,4]{1,0:T(4,128)S(1)}, f32[4,4,64,128]{3,2,1,0:T(8,128)...) while((s32[]{:T(128)}, f32[4,128,128]{2,1,0:T(8,128)S(1)}, ...), condition=%wide.region_17.18_spmd, body=%wide.region_16.17_spmd.sunk | while | flops 176357376 | bytes 2493593 | solution.py:305
  222.8 1.9 fusion.203
  232.2 3.4 convolution_convert_fusion.3
  237.5 2.2 copy.91
  239.6 6.6 %collective-permute-done.1 = bf16[256,512]{1,0:T(8,128)(2,1)} collective-permute-done((bf16[256,512]{1,0:T(8,128)(2,1)}, bf16[256,512]{1,0:T(8,128)(2,1)}, u32[]{:S(2)}, u32[]{:S(2)}) %collective-permute-start.1) | collective-permute-done | bytes 262176 | tf_op jit(solution)/shard_map/ppermute | solution.py:279
  246.3 3.0 convolution_convert_fusion.4
  251.1 3.7 %collective-permute-done.2 = bf16[256,512]{1,0:T(8,128)(2,1)} collective-permute-done((bf16[256,512]{1,0:T(8,128)(2,1)}, bf16[256,512]{1,0:T(8,128)(2,1)}, u32[]{:S(2)}, u32[]{:S(2)}) %collective-permute-start.2) | collective-permute-done | bytes 262176 | tf_op jit(solution)/shard_map/ppermute | solution.py:279
  262.2 11.1 %all-gather.18.cloned.1.call-done = bf16[1024,512]{1,0:T(8,128)(2,1)} async-done(((bf16[256,512]{1,0:T(8,128)(2,1)}), bf16[1024,512]{1,0:T(8,128)(2,1)}) %all-gather.18.cloned.1.call-update) | async-done | bytes 1048592 | tf_op jit(solution)/shard_map/all_gather | solution.py:283
  273.3 2.3 copy.81
  277.8 14.7 %while.59 = (s32[]{:T(128)}, f32[4,256,8,64]{1,3,2,0:T(8,128)}, f32[4,256,8]{1,2,0:T(8,128)}, s32[]{:T(128)}, bf16[1024,512]{0,1:T(8,128)(2,1)}, /*index=5*/bf16...) while((s32[]{:T(128)}, f32[4,256,8,64]{1,3,2,0:T(8,128)}, ...), condition=%wide.region_6.7_spmd.clone.clone, body=%wide.region_0.6_spmd.clone.clone.sunk | while | flops 218698256 | bytes 25745960 | solution.py:294
  277.8 14.7 %conditional.4 = ((f32[4,256,8,64]{1,3,2,0:T(8,128)}, f32[4,256,8]{1,2,0:T(8,128)})) conditional(s32[]{:T(128)} %convert_element_type.140, (f32[4,256,8,64]{1,3,2,0:T(8,128)}, f32[4,256,8]{1,2,0:T(8,128)}) %tuple.124, (s32[]{:T(128)}, s32[]{:T(128)}, bf16[1024,512]{0,1:T(8,128)(2,1)}, bf16[256,8,64]{0,2,1:T(8,128)(2,1)}, f32[8]{0:T(128)S(1)}, ...), branch_computations={%region_1.1_spmd, %region_2.0_spmd} | conditional | flops 218698256 | bytes 25744700 | solution.py:274
  279.0 2.7 fusion.17
  281.7 5.1 %fusion.13 = f32[8,256,2,128]{1,0,3,2:T(8,128)S(1)} fusion(f32[8,256,2,128]{1,3,2,0:T(8,128)S(1)} %bitcast.258), kind=kOutput, calls=%fused_computation.18 | output fusion | flops 66584576 | bytes 4194304 | tf_op jit(solution)/shard_map/reduce-window.6
  287.7 3.0 fusion.6
  299.6 51.9 %reduce-scatter.2.cloned.1.call-done = bf16[128,2048]{1,0:T(8,128)(2,1)} async-done(((bf16[256,2048]{1,0:T(8,128)(2,1)}), bf16[128,2048]{1,0:T(8,128)(2,1)}) %reduce-scatter.2.cloned.1.call-update) | async-done | bytes 524304 | tf_op jit(solution)/shard_map/reduce_scatter | solution.py:313
  (190 shorter events, 98.1 us)
Async XLA Ops:
  6.5 289.5 %copy-start = (bf16[512,2048]{1,0:T(8,128)(2,1)S(1)}, bf16[512,2048]{1,0:T(8,128)(2,1)}, u32[]{:S(2)}) copy-start(bf16[512,2048]{1,0:T(8,128)(2,1)} %param.40) | copy-start | bytes 6291460
  6.5 4.9 %copy-start.15 = (f32[4]{0:T(128)S(1)}, f32[4]{0:T(128)}, u32[]{:S(2)}) copy-start(f32[4]{0:T(128)} %param.37) | copy-start | bytes 52
  6.5 4.9 %copy-start.14 = (f32[128]{0:T(128)S(1)}, f32[128]{0:T(128)}, u32[]{:S(2)}) copy-start(f32[128]{0:T(128)} %param.39) | copy-start | bytes 1540
  6.5 14.1 %copy-start.8 = (bf16[2048,4]{0,1:T(4,128)(2,1)S(1)}, bf16[2048,4]{0,1:T(4,128)(2,1)}, u32[]{:S(2)}) copy-start(bf16[2048,4]{0,1:T(4,128)(2,1)} %param.34) | copy-start | bytes 49156
  6.5 14.1 %copy-start.12 = (f32[1,4,256]{2,1,0:T(4,128)S(1)}, f32[1,4,256]{2,1,0:T(4,128)}, u32[]{:S(2)}) copy-start(f32[1,4,256]{2,1,0:T(4,128)} %param.38) | copy-start | bytes 12292
  6.5 14.1 %all-gather.26.cloned.1.call-start = ((), (), s32[]{:S(2)}) async-start(), calls=%async_computation.9 | async-start | bytes 1572864 | tf_op jit(solution)/shard_map/all_gather | solution.py:211
  7.3 51.6 %all-gather.20.cloned.1.call-start = ((), (), s32[]{:S(2)}) async-start(), calls=%async_computation.5 | async-start | bytes 2621440 | tf_op jit(solution)/shard_map/all_gather | solution.py:207
  8.0 15.6 %copy-start.9 = (bf16[2048,4]{0,1:T(4,128)(2,1)S(1)}, bf16[2048,4]{0,1:T(4,128)(2,1)}, u32[]{:S(2)}) copy-start(bf16[2048,4]{0,1:T(4,128)(2,1)} %param.35) | copy-start | bytes 49156
  8.0 15.6 %copy-start.13 = (f32[4]{0:T(128)S(1)}, f32[4]{0:T(128)}, u32[]{:S(2)}) copy-start(f32[4]{0:T(128)} %param.36) | copy-start | bytes 52
  8.1 87.9 %all-gather.22.cloned.1.call-start = ((), (), s32[]{:S(2)}) async-start(), calls=%async_computation.6 | async-start | bytes 2621440 | tf_op jit(solution)/shard_map/all_gather | solution.py:208
  8.8 124.1 %all-gather.24.cloned.1.call-start = ((), (), s32[]{:S(2)}) async-start(), calls=%async_computation.7 | async-start | bytes 2621440 | tf_op jit(solution)/shard_map/all_gather | solution.py:206
  9.4 195.5 %all-gather.12.cloned.1.call-start = ((), (), s32[]{:S(2)}) async-start(), calls=%async_computation.1 | async-start | bytes 2621440 | tf_op jit(solution)/shard_map/all_gather | solution.py:204
  10.0 222.3 %all-gather.16.cloned.1.call-start = ((), (), s32[]{:S(2)}) async-start(), calls=%async_computation.3 | async-start | bytes 2621440 | tf_op jit(solution)/shard_map/all_gather | solution.py:205
  10.5 235.7 %all-gather.14.cloned.1.call-start = ((), (), s32[]{:S(2)}) async-start(), calls=%async_computation.2 | async-start | bytes 2621440 | tf_op jit(solution)/shard_map/all_gather | solution.py:203
  11.3 262.0 %all-gather.18.cloned.1.call-start = ((), (), s32[]{:S(2)}) async-start(), calls=%async_computation.4 | async-start | bytes 1310720 | tf_op jit(solution)/shard_map/all_gather | solution.py:283
  65.5 2.6 copy-start.1
  101.5 4.0 %copy-start.5 = (f32[4,64,4,128]{3,2,1,0:T(4,128)S(1)}, f32[4,64,4,128]{3,2,1,0:T(4,128)}, u32[]{:S(2)}) copy-start(f32[4,64,4,128]{3,2,1,0:T(4,128)} %reshape_reshape.3) | copy-start | bytes 1572868
  142.3 3.4 copy-start.2
  142.3 3.4 copy-start.7
  207.5 28.1 %collective-permute-start = (bf16[256,512]{1,0:T(8,128)(2,1)S(1)}, bf16[256,512]{1,0:T(8,128)(2,1)}, u32[]{:S(2)}, u32[]{:S(2)}) collective-permute-start(bf16[256,512]{1,0:T(8,128)(2,1)S(1)} %convolution_convert_fusion.5), channel_id=1, source_target_pairs={{0,8},{8,16},{16,24},{24,0},{1,9},{9,17},{17,25},{25,1},{2,10},{10... | collective-permute-start | bytes 786440 | tf_op jit(solution)/shard_map/ppermute | solution.py:279
  232.2 14.1 %copy-start.3 = (bf16[1,256,2048]{2,1,0:T(8,128)(2,1)S(1)}, bf16[1,256,2048]{2,1,0:T(8,128)(2,1)}, u32[]{:S(2)}) copy-start(bf16[1,256,2048]{2,1,0:T(8,128)(2,1)} %all-gather.26.cloned.1.call-done) | copy-start | bytes 3145732
  235.6 10.6 %collective-permute-start.1 = (bf16[256,512]{1,0:T(8,128)(2,1)}, bf16[256,512]{1,0:T(8,128)(2,1)}, u32[]{:S(2)}, u32[]{:S(2)}) collective-permute-start(bf16[256,512]{1,0:T(8,128)(2,1)} %collective-permute-done), channel_id=1, source_target_pairs={{0,8},{8,16},{16,24},{24,0},{1,9},{9,17},{17,25},{25,1},{2,10},{10... | collective-permute-start | bytes 786440 | tf_op jit(solution)/shard_map/ppermute | solution.py:279
  237.3 114.3 %reduce-scatter.2.cloned.1.call-start = ((), (), s32[]{:S(2)}) async-start(), calls=%async_computation.8 | async-start | bytes 1572864 | tf_op jit(solution)/shard_map/reduce_scatter | solution.py:313
  246.2 8.5 %collective-permute-start.2 = (bf16[256,512]{1,0:T(8,128)(2,1)}, bf16[256,512]{1,0:T(8,128)(2,1)}, u32[]{:S(2)}, u32[]{:S(2)}) collective-permute-start(bf16[256,512]{1,0:T(8,128)(2,1)} %collective-permute-done.1), channel_id=1, source_target_pairs={{0,8},{8,16},{16,24},{24,0},{1,9},{9,17},{17,25},{25,1},{2,10},{10... | collective-permute-start | bytes 786440 | tf_op jit(solution)/shard_map/ppermute | solution.py:279
  262.2 15.5 %copy-start.10 = (f32[8]{0:T(128)S(1)}, f32[8]{0:T(128)}, u32[]{:S(2)}) copy-start(f32[8]{0:T(128)} %param.30) | copy-start | bytes 100
  296.1 1.1 copy-start.4
  296.1 1.8 copy-start.6
  296.1 1.8 copy-start.11
Sparse Core Ops, SparseCore 0:
  8.9 11.7 all-gather.25
  22.5 36.3 all-gather.19
  60.8 35.1 all-gather.21
  97.7 35.1 all-gather.23
  134.6 35.1 all-gather.11
  171.5 35.1 all-gather.15
  208.5 35.1 all-gather.13
  245.3 27.9 all-gather.17
  299.8 51.7 reduce-scatter.1
